TPU v7x, 512 devices: a whole 4x4x16 slice. The times are simulated.
512 devices in a mesh: ep: 16 (over y, x), tp: 32 (over z, core).
Axes of the slice: x: 4, y: 4, z: 16, core: 2. Of those that a mesh axis runs over, the one named last changes fastest.
Arguments:
- tokens: bfloat16 [2048, 4096], P('ep', 'tp'), may hold values from -16 to 16
- routing: int32 [2048, 4], P('ep'), may hold values from 0 to 31, all different within a row; in each aligned block of 128 rows (0 to 127, 128 to 255, ...) at most 32 rows name the same one
- gate_weights: float32 [2048, 4], P('ep'), may hold values from 0.1 to 1
- w_gate: bfloat16 [32, 1024, 4096], P('ep', 'tp'), may hold values from -0.09375 to 0.09375
- w_up: bfloat16 [32, 1024, 4096], P('ep', 'tp'), may hold values from -0.09375 to 0.09375
- w_down: bfloat16 [32, 1024, 4096], P('ep', None, 'tp'), may hold values from -2 to 2
- out_gain: float32 [4096], P('tp'), may hold values from 0.1 to 1.9
Outputs:
- mixed: bfloat16 [2048, 4096], P('ep', 'tp')
Inputs may be any that keep to these rules, and one draw needn't show every extreme that they name: `routing`: in each aligned block of 128 rows (the tokens of one index of ep) no expert is named by more than 32 entries, and in every draw some expert is named by exactly 32 entries of some block. The 4 entries of a row differ.
All inputs are finite; a program needn't handle non-finite values.
Results may differ from a plain program's by a relative error of at most 0.0057.
Values may be sent and summed in bfloat16 or wider, within the bound.
A program may use at most 64 MiB of HBM per device.

v0:
```python
import jax
import jax.numpy as jnp
from jax import lax
from jax.sharding import PartitionSpec as P

D = 4096
TOPK = 4
EXP_DEV = 2
norm_eps = 1e-05


def from_everyone(value, axis):
    length = lax.axis_size(axis)
    return lax.all_to_all(
        jnp.broadcast_to(value[None], (length, *value.shape)), axis, 0, 0, tiled=True
    )


def taken_together(value, axis):
    return from_everyone(value, axis).sum(axis=0)


def body(tokens, routing, gate_weights, w_gate, w_up, w_down, out_gain):
    ep_count = lax.axis_size("ep")
    tok_rows = tokens.shape[0]
    width_part = tokens.shape[1]
    experts = EXP_DEV * ep_count
    slot_count = 2 * tok_rows * TOPK // experts
    span_rows = ep_count * slot_count
    total_slots = EXP_DEV * span_rows
    flat_route = routing.reshape(-1)
    expert_ids = jnp.arange(experts, dtype=jnp.int32)
    hit_table = (flat_route[:, None] == expert_ids[None, :]).astype(jnp.int32)
    running = jnp.cumsum(hit_table, axis=0) - hit_table
    slot_rank = jnp.sum(running * hit_table, axis=1)
    slot_target = flat_route % EXP_DEV * span_rows + flat_route // EXP_DEV * slot_count + slot_rank
    entry_targets = slot_target.reshape(tok_rows, TOPK)
    slot_ids = jnp.arange(total_slots, dtype=jnp.int32)
    select_table = jnp.any(entry_targets[None, :, :] == slot_ids[:, None, None], axis=2).astype(
        jnp.bfloat16
    )
    outgoing = jnp.dot(select_table, tokens, preferred_element_type=jnp.float32).astype(
        jnp.bfloat16
    )
    outgoing = outgoing.reshape(EXP_DEV, ep_count, slot_count, width_part)
    arrived = lax.all_to_all(outgoing, "ep", split_axis=1, concat_axis=1, tiled=True).reshape(
        EXP_DEV, span_rows, width_part
    )
    piece_cols = lax.all_gather(arrived, "tp", axis=2, tiled=True)
    gate_sum = jnp.einsum("efn,esn->efs", w_gate, piece_cols, preferred_element_type=jnp.float32)
    up_sum = jnp.einsum("efn,esn->efs", w_up, piece_cols, preferred_element_type=jnp.float32)
    square_sum = jnp.einsum(
        "esn,esn->es", piece_cols, piece_cols, preferred_element_type=jnp.float32
    )
    row_scale = lax.rsqrt(square_sum / D + norm_eps)[:, None, :]
    hidden = (jax.nn.silu(gate_sum * row_scale) * (up_sum * row_scale)).astype(jnp.bfloat16)
    out_part = w_down.shape[2]
    expert_out = jnp.einsum(
        "ens,end->esd",
        lax.all_gather(hidden, "tp", axis=1, tiled=True),
        w_down,
        preferred_element_type=jnp.float32,
    ).astype(jnp.bfloat16)
    returned = lax.all_to_all(
        expert_out.reshape(EXP_DEV, ep_count, slot_count, out_part),
        "ep",
        split_axis=1,
        concat_axis=1,
        tiled=True,
    )
    returned = returned.reshape(total_slots, out_part)
    chosen = returned[slot_target].astype(jnp.float32).reshape(tok_rows, TOPK, out_part)
    combined = jnp.sum(chosen * gate_weights[:, :, None], axis=1)
    square_total = taken_together(jnp.sum(combined * combined, axis=1), "tp")
    final_scale = lax.rsqrt(square_total / D + norm_eps)
    return (combined * final_scale[:, None] * out_gain[None, :]).astype(jnp.bfloat16)


def solution(mesh):
    placed = (
        P("ep", "tp"),
        P("ep", None),
        P("ep", None),
        P("ep", "tp", None),
        P("ep", "tp", None),
        P("ep", None, "tp"),
        P("tp"),
    )
    return jax.shard_map(body, mesh=mesh, in_specs=placed, out_specs=P("ep", "tp"), check_vma=False)
```

profile of v0, /device:TPU:1, one launch (start us, length us, event | category | flops | bytes accessed | tf_op | source)
XLA Modules:
  0.0 253.4 jit_solution(5410838036807146994)
XLA Ops:
  6.5 0.9 copy.73
  7.6 1.2 reduce-window.6
  8.8 0.2 slice_reduce_fusion
  9.2 0.1 reduce_sum.41
  9.4 0.7 fusion.13
  10.1 0.4 fusion.1
  10.4 1.0 convolution_convert_fusion.1
  11.5 14.9 %all_to_all.16 = bf16[2,16,32,128]{3,2,0,1:T(8,128)(2,1)S(1)} all-to-all(bf16[2,16,32,128]{3,2,0,1:T(8,128)(2,1)S(1)} %copy.77), channel_id=1, replica_groups=mesh['ep'=16,'tp'=32] {'ep'}, dimensions={1} | all-to-all | bytes 524288 | tf_op jit(solution)/shard_map/all_to_all | solution.py:46
  26.4 0.7 copy.78
  27.2 98.1 %all-gather.3.cloned.1.call-done = bf16[2,512,4096]{2,1,0:T(8,128)(2,1)} async-done(((bf16[2,512,128]{2,1,0:T(8,128)(2,1)}), bf16[2,512,4096]{2,1,0:T(8,128)(2,1)}) %all-gather.3.cloned.1.call-update) | async-done | bytes 8388624 | tf_op jit(solution)/shard_map/all_gather | solution.py:49
  125.2 5.2 %fusion = f32[2,512]{1,0:T(2,128)S(1)} fusion(bf16[2,512,4096]{2,1,0:T(8,128)(2,1)} %all-gather.3.cloned.1.call-done), kind=kLoop, calls=%fused_computation.2 | loop fusion | flops 12581888 | bytes 8392704 | tf_op jit(solution)/shard_map/esn,esn->es/dot_general | solution.py:52
  130.5 0.5 copy-done.1
  131.0 2.6 %fusion.3 = f32[2,32,512]{2,1,0:T(8,128)S(1)} fusion(bf16[2,512,4096]{2,1,0:T(8,128)(2,1)S(1)} %copy-done.1, bf16[2,32,4096]{2,1,0:T(8,128)(2,1)S(1)} %copy-done.2, f32[2,512]{1,0:T(2,128)S(1)} %add_rsqrt_fusion), kind=kOutput, calls=%fused_computation.10 | convolution fusion | flops 268468224 | bytes 9048064 | tf_op jit(solution)/shard_map/efn,esn->efs/dot_general | solution.py:50
  133.7 3.2 %fusion.5 = bf16[2,32,512]{2,1,0:T(8,128)(2,1)} fusion(bf16[2,512,4096]{2,1,0:T(8,128)(2,1)S(1)} %copy-done.1, bf16[2,32,4096]{2,1,0:T(8,128)(2,1)S(1)} %copy-done.3, f32[2,32,512]{2,1,0:T(8,128)S(1)} %fusion.3, f32[2,512]{1,0:T(2,128)S(1)} %add_rsqrt_fusion), kind=kOutput, calls=%fused_computation.12 | convolution fusion | flops 268664832 | bytes 9113600 | tf_op jit(solution)/shard_map/efn,esn->efs/dot_general | solution.py:51
  137.0 0.1 copy.82
  137.2 67.7 %all-gather.5.cloned.1.call-done = bf16[2,1024,512]{2,1,0:T(8,128)(2,1)} async-done(((bf16[2,32,512]{2,1,0:T(8,128)(2,1)}), bf16[2,1024,512]{2,1,0:T(8,128)(2,1)}) %all-gather.5.cloned.1.call-update) | async-done | bytes 2097168 | tf_op jit(solution)/shard_map/all_gather | solution.py:60
  204.9 2.5 convolution_convert_fusion
  207.4 0.7 copy.79
  208.1 6.5 %all-to-all-start.1 = ((bf16[2,16,32,128]{3,2,0,1:T(8,128)(2,1)}), bf16[2,16,32,128]{3,2,0,1:T(8,128)(2,1)S(1)}, u32[]{:S(2)}, u32[]{:S(2)}) async-start(bf16[2,16,32,128]{3,2,0,1:T(8,128)(2,1)} %copy.79), calls=%async_computation.1 | async-start | bytes 524288 | tf_op jit(solution)/shard_map/all_to_all | solution.py:64
  214.7 8.2 %all-to-all-done.1 = bf16[2,16,32,128]{3,2,0,1:T(8,128)(2,1)S(1)} async-done(((bf16[2,16,32,128]{3,2,0,1:T(8,128)(2,1)}), bf16[2,16,32,128]{3,2,0,1:T(8,128)(2,1)S(1)}, u32[]{:S(2)}, u32[]{:S(2)}) %all-to-all-start.1) | async-done | bytes 262176 | tf_op jit(solution)/shard_map/all_to_all | solution.py:64
  222.9 1.3 gather_fusion
  224.2 0.2 fusion.6
  224.6 21.2 %all_to_all.17 = f32[32,1,128]{2,1,0:T(1,128)S(1)} all-to-all(f32[32,1,128]{2,1,0:T(1,128)S(1)} %broadcast_in_dim.2), channel_id=1, replica_groups=mesh['ep'=16,'tp'=32] {'tp'}, dimensions={0} | all-to-all | bytes 32768 | tf_op jit(solution)/shard_map/all_to_all | solution.py:14
  245.9 0.7 multiply_convert_fusion
  (32 shorter events, 0.9 us)
Async XLA Ops:
  6.5 198.4 %copy-start = (bf16[2,1024,128]{2,1,0:T(8,128)(2,1)S(1)}, bf16[2,1024,128]{2,1,0:T(8,128)(2,1)}, u32[]{:S(2)}) copy-start(bf16[2,1024,128]{2,1,0:T(8,128)(2,1)} %param.12) | copy-start | bytes 1572868
  6.5 124.0 %copy-start.2 = (bf16[2,32,4096]{2,1,0:T(8,128)(2,1)S(1)}, bf16[2,32,4096]{2,1,0:T(8,128)(2,1)}, u32[]{:S(2)}) copy-start(bf16[2,32,4096]{2,1,0:T(8,128)(2,1)} %param.10) | copy-start | bytes 1572868
  6.5 118.7 %all-gather.3.cloned.1.call-start = ((), (), s32[]{:S(2)}) async-start(), calls=%async_computation.3 | async-start | bytes 8650752 | tf_op jit(solution)/shard_map/all_gather | solution.py:49
  27.1 177.8 %all-gather.5.cloned.1.call-start = ((), (), s32[]{:S(2)}) async-start(), calls=%async_computation.4 | async-start | bytes 2162688 | tf_op jit(solution)/shard_map/all_gather | solution.py:60
  125.2 5.8 %copy-start.1 = (bf16[2,512,4096]{2,1,0:T(8,128)(2,1)S(1)}, bf16[2,512,4096]{2,1,0:T(8,128)(2,1)}, u32[]{:S(2)}) copy-start(bf16[2,512,4096]{2,1,0:T(8,128)(2,1)} %all-gather.3.cloned.1.call-done) | copy-start | bytes 25165828
  125.2 8.4 %copy-start.3 = (bf16[2,32,4096]{2,1,0:T(8,128)(2,1)S(1)}, bf16[2,32,4096]{2,1,0:T(8,128)(2,1)}, u32[]{:S(2)}) copy-start(bf16[2,32,4096]{2,1,0:T(8,128)(2,1)} %param.11) | copy-start | bytes 1572868
  131.0 6.0 %copy-start.4 = (f32[128,4]{0,1:T(4,128)S(1)}, f32[128,4]{0,1:T(4,128)}, u32[]{:S(2)}) copy-start(f32[128,4]{0,1:T(4,128)} %param.9) | copy-start | bytes 6148
  133.7 112.2 %copy-start.5 = (f32[128]{0:T(128)S(1)}, f32[128]{0:T(128)}, u32[]{:S(2)}) copy-start(f32[128]{0:T(128)} %param.13) | copy-start | bytes 1540
  208.1 14.7 %all-to-all-start.1 = ((bf16[2,16,32,128]{3,2,0,1:T(8,128)(2,1)}), bf16[2,16,32,128]{3,2,0,1:T(8,128)(2,1)S(1)}, u32[]{:S(2)}, u32[]{:S(2)}) async-start(bf16[2,16,32,128]{3,2,0,1:T(8,128)(2,1)} %copy.79), calls=%async_computation.1 | async-start | bytes 524288 | tf_op jit(solution)/shard_map/all_to_all | solution.py:64
Sparse Core Ops, SparseCore 0:
  27.2 97.9 all-gather.2
  137.0 67.7 all-gather.4
where the time goes:
time: 254 us; the launch traced here: 253 us
  waiting for transfers between devices  174 us (69%)
  blocking collectives  36.1 us (14%)
  between operations  13.5 us (5%)
  matrix products  9.35 us (4%)
  other arithmetic  8.73 us (3%)
  starting transfers between devices  6.57 us (3%)
  local copies, waits for them, and re-layouts  5.09 us (2%)
    all_gather x1, waiting for transfers between devices, body(): piece_cols = lax.all_gather(arrived, 'tp', axis=2, tiled=True)  98.1 us
    all_gather x1, waiting for transfers between devices, body(): lax.all_gather(hidden, 'tp', axis=1, tiled=True)  67.7 us
    all_to_all x1, blocking collectives, from_everyone(): lax.all_to_all(jnp.broadcast_to(value[None], (length, *value.shape)), axi...  21.2 us
    all_to_all x1, blocking collectives, body(): lax.all_to_all(outgoing, 'ep', split_axis=1, concat_axis=1, tiled=True)  14.9 us
    all_to_all x1, waiting for transfers between devices, body(): lax.all_to_all(expert_out.reshape(EXP_DEV, ep_count, slot_count, out_part...  8.16 us
    all_to_all x1, starting transfers between devices, body(): lax.all_to_all(expert_out.reshape(EXP_DEV, ep_count, slot_count, out_part...  6.53 us
    dot_general x1, other arithmetic, body(): jnp.einsum('esn,esn->es', piece_cols, piece_cols, preferred_element_type=...  5.23 us
  transfers between devices with their start and end apart: 3, of which 3 were waited for; matrix products, arithmetic and copies ran while one was open for 0% of the time, Pallas kernels for 0%

commit v1 on v0

--- a/solution.py
+++ b/solution.py
@@ -46,7 +46,7 @@
     arrived = lax.all_to_all(outgoing, "ep", split_axis=1, concat_axis=1, tiled=True).reshape(
         EXP_DEV, span_rows, width_part
     )
-    piece_cols = lax.all_gather(arrived, "tp", axis=2, tiled=True)
+    piece_cols = jnp.concatenate(lax.all_gather(arrived, "tp"), 2)
     gate_sum = jnp.einsum("efn,esn->efs", w_gate, piece_cols, preferred_element_type=jnp.float32)
     up_sum = jnp.einsum("efn,esn->efs", w_up, piece_cols, preferred_element_type=jnp.float32)
     square_sum = jnp.einsum(

time: 254 us -> 237 us (0.933)
  waiting for transfers between devices: 174 us -> 158 us
    all_gather x1, waiting for transfers between devices: 98.1 us -> 81.2 us  [body(): piece_cols = jnp.concatenate(lax.all_gather(arrived, 'tp'), 2)]
where the time goes in v1:
time: 237 us
  waiting for transfers between devices  158 us (67%)
  blocking collectives  36.1 us (15%)
  between operations  13.5 us (6%)
  matrix products  9.17 us (4%)
  other arithmetic  8.73 us (4%)
  starting transfers between devices  6.57 us (3%)
  local copies, waits for them, and re-layouts  5.09 us (2%)
    all_gather x1, waiting for transfers between devices, body(): piece_cols = jnp.concatenate(lax.all_gather(arrived, 'tp'), 2)  81.2 us
    all_gather x1, waiting for transfers between devices, body(): lax.all_gather(hidden, 'tp', axis=1, tiled=True)  68.1 us
    all_to_all x1, blocking collectives, from_everyone(): lax.all_to_all(jnp.broadcast_to(value[None], (length, *value.shape)), axi...  21.2 us
    all_to_all x1, blocking collectives, body(): lax.all_to_all(outgoing, 'ep', split_axis=1, concat_axis=1, tiled=True)  14.9 us
    all_to_all x1, waiting for transfers between devices, body(): lax.all_to_all(expert_out.reshape(EXP_DEV, ep_count, slot_count, out_part...  8.16 us
    all_to_all x1, starting transfers between devices, body(): lax.all_to_all(expert_out.reshape(EXP_DEV, ep_count, slot_count, out_part...  6.53 us
    dot_general x1, other arithmetic, body(): jnp.einsum('esn,esn->es', piece_cols, piece_cols, preferred_element_type=...  5.23 us
  transfers between devices with their start and end apart: 3, of which 3 were waited for; matrix products, arithmetic and copies ran while one was open for 0% of the time, Pallas kernels for 0%

profile of v1, /device:TPU:1, one launch (start us, length us, event | category | flops | bytes accessed | tf_op | source)
XLA Modules:
  0.0 236.8 jit_solution(8803433938441525516)
XLA Ops:
  6.5 0.9 copy.94
  7.6 1.2 reduce-window.6
  8.8 0.2 slice_reduce_fusion
  9.2 0.1 reduce_sum.41
  9.4 0.7 fusion.33
  10.1 0.4 fusion.7
  10.4 1.0 convolution_convert_fusion.1
  11.5 14.9 %all_to_all.16 = bf16[2,16,32,128]{3,2,0,1:T(8,128)(2,1)S(1)} all-to-all(bf16[2,16,32,128]{3,2,0,1:T(8,128)(2,1)S(1)} %copy.98), channel_id=1, replica_groups=mesh['ep'=16,'tp'=32] {'ep'}, dimensions={1} | all-to-all | bytes 524288 | tf_op jit(solution)/shard_map/all_to_all | solution.py:46
  26.4 0.7 copy.99
  27.2 81.2 %all-gather.3.cloned.1.call-done = bf16[32,2,512,128]{3,2,1,0:T(8,128)(2,1)} async-done(((bf16[1,2,512,128]{3,2,1,0:T(8,128)(2,1)}), bf16[32,2,512,128]{3,2,1,0:T(8,128)(2,1)}) %all-gather.3.cloned.1.call-update) | async-done | bytes 8388624 | tf_op jit(solution)/shard_map/all_gather | solution.py:49
  108.4 5.2 %fusion = f32[2,512]{1,0:T(2,128)S(1)} fusion(bf16[32,2,512,128]{3,2,1,0:T(8,128)(2,1)} %all-gather.3.cloned.1.call-done), kind=kLoop, calls=%fused_computation.2 | loop fusion | flops 12581888 | bytes 8392704 | tf_op jit(solution)/shard_map/esn,esn->es/dot_general | solution.py:52
  113.7 0.5 copy-done.1
  114.2 2.5 %fusion.11 = f32[2,32,512]{2,1,0:T(8,128)S(1)} fusion(bf16[2,32,4096]{2,1,0:T(8,128)(2,1)S(1)} %copy-done.4, f32[2,512]{1,0:T(2,128)S(1)} %add_rsqrt_fusion, bf16[32,2,512,128]{3,2,1,0:T(8,128)(2,1)S(1)} %copy-done.1), kind=kOutput, calls=%fused_computation.14 | convolution fusion | flops 268468224 | bytes 9048064 | tf_op jit(solution)/shard_map/efn,esn->efs/dot_general | solution.py:50
  116.7 3.2 %fusion.23 = bf16[2,32,512]{2,1,0:T(8,128)(2,1)} fusion(bf16[2,32,4096]{2,1,0:T(8,128)(2,1)S(1)} %copy-done.5, f32[2,32,512]{2,1,0:T(8,128)S(1)} %fusion.11, f32[2,512]{1,0:T(2,128)S(1)} %add_rsqrt_fusion, bf16[32,2,512,128]{3,2,1,0:T(8,128)(2,1)S(1)} %copy-done.1), kind=kOutput, calls=%fused_computation.18 | convolution fusion | flops 268664832 | bytes 9113600 | tf_op jit(solution)/shard_map/efn,esn->efs/dot_general | solution.py:51
  120.0 0.1 copy.104
  120.2 68.1 %all-gather.5.cloned.1.call-done = bf16[2,1024,512]{2,1,0:T(8,128)(2,1)} async-done(((bf16[2,32,512]{2,1,0:T(8,128)(2,1)}), bf16[2,1024,512]{2,1,0:T(8,128)(2,1)}) %all-gather.5.cloned.1.call-update) | async-done | bytes 2097168 | tf_op jit(solution)/shard_map/all_gather | solution.py:60
  188.2 2.5 %convolution_convert_fusion = bf16[2,512,128]{2,1,0:T(8,128)(2,1)S(1)} fusion(bf16[2,1024,512]{2,1,0:T(8,128)(2,1)} %all-gather.5.cloned.1.call-done, bf16[2,1024,128]{2,1,0:T(8,128)(2,1)S(1)} %copy-done), kind=kOutput, calls=%fused_computation.11 | convolution fusion | flops 268566528 | bytes 2883584 | tf_op jit(solution)/shard_map/ens,end->esd/dot_general | solution.py:58
  190.8 0.7 copy.101
  191.5 6.5 %all-to-all-start.1 = ((bf16[2,16,32,128]{3,2,0,1:T(8,128)(2,1)}), bf16[2,16,32,128]{3,2,0,1:T(8,128)(2,1)S(1)}, u32[]{:S(2)}, u32[]{:S(2)}) async-start(bf16[2,16,32,128]{3,2,0,1:T(8,128)(2,1)} %copy.101), calls=%async_computation.1 | async-start | bytes 524288 | tf_op jit(solution)/shard_map/all_to_all | solution.py:64
  198.1 8.2 %all-to-all-done.1 = bf16[2,16,32,128]{3,2,0,1:T(8,128)(2,1)S(1)} async-done(((bf16[2,16,32,128]{3,2,0,1:T(8,128)(2,1)}), bf16[2,16,32,128]{3,2,0,1:T(8,128)(2,1)S(1)}, u32[]{:S(2)}, u32[]{:S(2)}) %all-to-all-start.1) | async-done | bytes 262176 | tf_op jit(solution)/shard_map/all_to_all | solution.py:64
  206.2 1.3 gather_fusion
  207.6 0.2 fusion.26
  208.0 21.2 %all_to_all.17 = f32[32,1,128]{2,1,0:T(1,128)S(1)} all-to-all(f32[32,1,128]{2,1,0:T(1,128)S(1)} %broadcast_in_dim.2), channel_id=1, replica_groups=mesh['ep'=16,'tp'=32] {'tp'}, dimensions={0} | all-to-all | bytes 32768 | tf_op jit(solution)/shard_map/all_to_all | solution.py:14
  229.2 0.7 multiply_convert_fusion
  (32 shorter events, 0.9 us)
Async XLA Ops:
  6.5 181.7 %copy-start = (bf16[2,1024,128]{2,1,0:T(8,128)(2,1)S(1)}, bf16[2,1024,128]{2,1,0:T(8,128)(2,1)}, u32[]{:S(2)}) copy-start(bf16[2,1024,128]{2,1,0:T(8,128)(2,1)} %param.12) | copy-start | bytes 1572868
  6.5 107.1 %copy-start.4 = (bf16[2,32,4096]{2,1,0:T(8,128)(2,1)S(1)}, bf16[2,32,4096]{2,1,0:T(8,128)(2,1)}, u32[]{:S(2)}) copy-start(bf16[2,32,4096]{2,1,0:T(8,128)(2,1)} %param.10) | copy-start | bytes 1572868
  6.5 101.9 %all-gather.3.cloned.1.call-start = ((), (), s32[]{:S(2)}) async-start(), calls=%async_computation.3 | async-start | bytes 8650752 | tf_op jit(solution)/shard_map/all_gather | solution.py:49
  27.1 161.1 %all-gather.5.cloned.1.call-start = ((), (), s32[]{:S(2)}) async-start(), calls=%async_computation.4 | async-start | bytes 2162688 | tf_op jit(solution)/shard_map/all_gather | solution.py:60
  108.4 5.8 %copy-start.1 = (bf16[32,2,512,128]{3,2,1,0:T(8,128)(2,1)S(1)}, bf16[32,2,512,128]{3,2,1,0:T(8,128)(2,1)}, u32[]{:S(2)}) copy-start(bf16[32,2,512,128]{3,2,1,0:T(8,128)(2,1)} %all-gather.3.cloned.1.call-done) | copy-start | bytes 25165828
  108.4 8.3 %copy-start.5 = (bf16[2,32,4096]{2,1,0:T(8,128)(2,1)S(1)}, bf16[2,32,4096]{2,1,0:T(8,128)(2,1)}, u32[]{:S(2)}) copy-start(bf16[2,32,4096]{2,1,0:T(8,128)(2,1)} %param.11) | copy-start | bytes 1572868
  116.7 3.3 %copy-start.2 = (f32[128,4]{0,1:T(4,128)S(1)}, f32[128,4]{0,1:T(4,128)}, u32[]{:S(2)}) copy-start(f32[128,4]{0,1:T(4,128)} %param.9) | copy-start | bytes 6148
  116.7 112.5 %copy-start.3 = (f32[128]{0:T(128)S(1)}, f32[128]{0:T(128)}, u32[]{:S(2)}) copy-start(f32[128]{0:T(128)} %param.13) | copy-start | bytes 1540
  191.5 14.7 %all-to-all-start.1 = ((bf16[2,16,32,128]{3,2,0,1:T(8,128)(2,1)}), bf16[2,16,32,128]{3,2,0,1:T(8,128)(2,1)S(1)}, u32[]{:S(2)}, u32[]{:S(2)}) async-start(bf16[2,16,32,128]{3,2,0,1:T(8,128)(2,1)} %copy.101), calls=%async_computation.1 | async-start | bytes 524288 | tf_op jit(solution)/shard_map/all_to_all | solution.py:64
Sparse Core Ops, SparseCore 0:
  27.2 81.1 all-gather.2
  120.0 68.1 all-gather.4
